TPU v7x, 256 devices: a 4x2x16 block of a 4x16x16 slice. The times are simulated.
256 devices in a mesh: grp: 2 (over y), fs: 16 (over z), tp: 8 (over x, core).
Axes of the slice: x: 4, y: 2, z: 16, core: 2. Of those that a mesh axis runs over, the one named last changes fastest.
The devices are a block of a 4x16x16 slice.
Arguments:
- tokens: bfloat16 [24576, 2048], P(('grp', 'fs'), 'tp'), parts along dimension 0, may hold values from -6 to 6
- mix_gain: float32 [2048], replicated, may hold values from 0.1 to 1.9
- w_u: float32 [2048, 1024], P('fs', 'tp'), may hold values from -0.125 to 0.125
- w_v: float32 [2048, 1024], P('fs', 'tp'), may hold values from -0.125 to 0.125
- u_scale: float32 [1024], P('tp'), may hold values from 0.5 to 2
- v_scale: float32 [1024], P('tp'), may hold values from 0.5 to 2
- spatial: bfloat16 [8, 128, 128], P('tp'), may hold values from -0.5 to 0.5
- spatial_bias: float32 [8, 128], P('tp'), may hold values from 0.1 to 1.9
- w_mix: float32 [1024, 2048], P('tp', 'fs'), may hold values from -0.1875 to 0.1875
- mix_scale: float32 [1, 2048], P(None, 'fs'), may hold values from 0.5 to 2
- ffn_gain: float32 [2048], replicated, may hold values from 0.1 to 1.9
- w_gate: float32 [2048, 5632], P('fs', 'tp'), may hold values from -0.125 to 0.125
- w_up: float32 [2048, 5632], P('fs', 'tp'), may hold values from -0.125 to 0.125
- gate_scale: float32 [5632], P('tp'), may hold values from 0.5 to 2
- up_scale: float32 [5632], P('tp'), may hold values from 0.5 to 2
- w_down: float32 [5632, 2048], P('tp', 'fs'), may hold values from -0.078125 to 0.078125
- down_scale: float32 [1, 2048], P(None, 'fs'), may hold values from 0.5 to 2
Outputs:
- layer_out: bfloat16 [24576, 2048], P(('grp', 'fs'), 'tp'), parts along dimension 0
There are 2 independent parts, one for each index of `grp`. A program takes and returns all parts, laid end to end along the dimension named above; an argument that names none is the same for every part. Nothing has to cross between parts.
All inputs are finite; a program needn't handle non-finite values.
Results may differ from a plain program's by a relative error of at most 0.024.
Values may be sent and summed in bfloat16 or wider, within the bound.
No kernel may reach another device: no remote copies, remote signals or barrier semaphores. Data moves between devices by JAX's collectives and lax.ppermute only.
A program may use at most 128 MiB of HBM per device.

v0:
```python
import jax
import jax.numpy as jnp
from jax import lax
from jax.sharding import PartitionSpec as P

eps = 1e-06


def sent_to_all(x, axis):
    count = lax.axis_size(axis)
    return lax.all_to_all(jnp.broadcast_to(x[None], (count, *x.shape)), axis, 0, 0, tiled=True)


def in_order(blocks, dim):
    lengths = list(blocks.shape[1:])
    lengths[dim] *= blocks.shape[0]
    return jnp.moveaxis(blocks, 0, dim).reshape(lengths)


def gather_directly(x, axis, dim):
    blocks = sent_to_all(x, axis)
    return in_order(blocks, dim)


def in_one_piece(arrays, axis, dim, along):
    both = jnp.concatenate(arrays, axis=along)
    out, at, done = (lax.all_gather(both, axis, axis=dim, tiled=True), 0, [])
    for a in arrays:
        done.append(lax.slice_in_dim(out, at, at + a.shape[along], axis=along))
        at += a.shape[along]
    return tuple(done)


def norm_rows(shard, gain):
    whole = gather_directly(shard, "tp", 1)
    wide = whole.astype(jnp.float32)
    factor = lax.rsqrt(jnp.mean(wide * wide, axis=1, keepdims=True) + eps)
    return (wide * factor * gain).astype(jnp.bfloat16)


def project_pair(rows, first, second):
    left = first.astype(jnp.bfloat16)
    right = second.astype(jnp.bfloat16)
    pieces = in_one_piece((left, right), "fs", 0, 1)
    return (
        jnp.dot(rows, pieces[0], preferred_element_type=jnp.float32),
        jnp.dot(rows, pieces[1], preferred_element_type=jnp.float32),
    )


def collect_out(weight, scale):
    return (
        lax.all_gather(weight.astype(jnp.bfloat16), "fs", axis=1, tiled=True),
        lax.all_gather(scale.astype(jnp.bfloat16), "fs", axis=1, tiled=True).astype(scale.dtype),
    )


def reduce_out(hidden, weight, scale):
    term = jnp.dot(hidden, weight, preferred_element_type=jnp.float32) * scale
    return lax.psum_scatter(
        term.astype(jnp.bfloat16), "tp", scatter_dimension=1, tiled=True
    ).astype(jnp.float32)


def local(
    tokens,
    mix_gain,
    w_u,
    w_v,
    u_scale,
    v_scale,
    spatial,
    spatial_bias,
    w_mix,
    mix_scale,
    ffn_gain,
    w_gate,
    w_up,
    gate_scale,
    up_scale,
    w_down,
    down_scale,
):
    held = collect_out(w_mix, mix_scale)
    normed_in = norm_rows(tokens, mix_gain)
    u_pre, v_pre = project_pair(normed_in, w_u, w_v)
    u_act = jax.nn.gelu(u_pre * u_scale, approximate=False)
    v_act = jax.nn.gelu(v_pre * v_scale, approximate=False).astype(jnp.bfloat16)
    groups = spatial.shape[0]
    span = spatial.shape[1]
    count = v_act.shape[0]
    blocks = v_act.reshape(count // span, span, groups, v_act.shape[1] // groups)
    later = lax.broadcasted_iota(jnp.int32, (span, span), 0)
    earlier = lax.broadcasted_iota(jnp.int32, (span, span), 1)
    masked = jnp.where((later >= earlier)[None], spatial, jnp.zeros((), jnp.bfloat16))
    spatial_out = jnp.einsum("gts,nsgc->ntgc", masked, blocks, preferred_element_type=jnp.float32)
    spatial_out = spatial_out + spatial_bias.T[None, :, :, None]
    gated = (u_act * spatial_out.reshape(count, v_act.shape[1])).astype(jnp.bfloat16)
    mixed = reduce_out(gated, held[0], held[1])
    resid = (tokens.astype(jnp.float32) + mixed).astype(jnp.bfloat16)
    down_weight, down_factor = collect_out(w_down, down_scale)
    normed_ffn = norm_rows(resid, ffn_gain)
    gate_pre, up_pre = project_pair(normed_ffn, w_gate, w_up)
    act = (jax.nn.silu(gate_pre * gate_scale) * (up_pre * up_scale)).astype(jnp.bfloat16)
    down_sum = reduce_out(act, down_weight, down_factor)
    return (resid.astype(jnp.float32) + down_sum).astype(jnp.bfloat16)


def solution(mesh):
    placed = (
        P(("grp", "fs"), "tp"),
        P(),
        P("fs", "tp"),
        P("fs", "tp"),
        P("tp"),
        P("tp"),
        P("tp", None, None),
        P("tp", None),
        P("tp", "fs"),
        P(None, "fs"),
        P(),
        P("fs", "tp"),
        P("fs", "tp"),
        P("tp"),
        P("tp"),
        P("tp", "fs"),
        P(None, "fs"),
    )
    return jax.shard_map(
        local, mesh=mesh, in_specs=placed, out_specs=P(("grp", "fs"), "tp"), check_vma=False
    )
```

profile of v0, /device:TPU:40, one launch (start us, length us, event | category | flops | bytes accessed | tf_op | source)
XLA Modules:
  0.0 392.7 jit_solution(11202266769531201021)
XLA Ops:
  6.5 1.2 copy.18
  7.7 1.8 broadcast_in_dim.7
  9.6 4.7 %all-to-all-start = ((bf16[8,768,256]{1,2,0:T(8,128)(2,1)}), bf16[8,768,256]{1,2,0:T(8,128)(2,1)S(1)}, u32[]{:S(2)}, u32[]{:S(2)}) async-start(bf16[8,768,256]{1,2,0:T(8,128)(2,1)} %broadcast_in_dim.7), calls=%async_computation | async-start | bytes 6291456 | tf_op jit(solution)/shard_map/all_to_all | solution.py:11
  14.3 0.1 all-gather.4.cloned.1.call-start
  14.4 0.0 copy-done.7
  14.4 0.0 copy-done.8
  14.4 0.6 pad_maximum_fusion.1
  15.1 0.1 all-gather.4.cloned.1.call-update
  15.1 0.1 reduce-scatter.3.cloned.1.call-start
  15.2 0.0 copy-done.17
  15.2 48.4 %all_gather.20 = bf16[1,2048]{1,0:T(2,128)(2,1)S(1)} all-gather(bf16[1,128]{1,0:T(2,128)(2,1)S(1)} %convert_element_type.102), channel_id=1, replica_groups=mesh['grp'=2,'fs'=16,'tp'=8] {'fs'}, dimensions={1}, use_global_device_ids=true | all-gather | bytes 4352 | tf_op jit(solution)/shard_map/all_gather | solution.py:54
  63.6 0.0 copy-done.9
  63.6 32.5 %all_gather.19 = bf16[128,2048]{1,0:T(8,128)(2,1)} all-gather(bf16[128,128]{1,0:T(8,128)(2,1)S(1)} %convert_element_type.101), channel_id=1, replica_groups=mesh['grp'=2,'fs'=16,'tp'=8] {'fs'}, dimensions={1}, use_global_device_ids=true | all-gather | bytes 557056 | tf_op jit(solution)/shard_map/all_gather | solution.py:53
  96.1 0.0 all-to-all-done
  96.1 0.7 multiply_reduce_fusion.1
  96.8 0.0 copy-done.11
  96.8 0.0 copy-start.18
  96.9 2.4 fusion.3
  99.3 0.3 all-gather.4.cloned.1.call-done
  99.6 0.0 copy-done.18
  99.6 3.9 fusion.21
  103.4 0.0 copy-done.10
  103.4 0.0 copy-done.13
  103.5 0.2 fusion.10
  103.7 0.0 copy-done.1
  103.7 0.0 copy-done.19
  103.7 0.0 copy-done.14
  103.7 0.0 copy-start.2
  103.7 1.7 fusion.18
  105.4 0.0 copy-done.2
  105.4 0.0 copy-start.4
  105.4 0.0 copy-start.5
  105.5 2.6 multiply_convert_fusion.1
  108.1 0.1 reduce-scatter.3.cloned.1.call-update
  108.2 0.1 all-gather.6.cloned.1.call-start
  108.2 0.0 copy-done.4
  108.3 0.0 copy-done.5
  108.3 0.8 pad_maximum_fusion
  109.1 0.1 all-gather.6.cloned.1.call-update
  109.1 0.1 all-gather.8.cloned.1.call-start
  109.2 0.0 copy-done.6
  109.2 0.7 convert_element_type.115
  109.9 0.1 all-gather.8.cloned.1.call-update
  110.0 37.4 %reduce-scatter.3.cloned.1.call-done = bf16[768,256]{1,0:T(8,128)(2,1)} async-done(((bf16[768,2048]{1,0:T(8,128)(2,1)}), bf16[768,256]{1,0:T(8,128)(2,1)}) %reduce-scatter.3.cloned.1.call-update) | async-done | bytes 393232 | tf_op jit(solution)/shard_map/reduce_scatter | solution.py:60
  147.4 0.0 copy-done.3
  147.4 1.1 add_convert_fusion.1
  148.5 0.2 copy.19
  148.7 1.9 broadcast_in_dim.9
  150.6 4.0 %all-to-all-start.1 = ((bf16[8,768,256]{1,2,0:T(8,128)(2,1)}), bf16[8,768,256]{1,2,0:T(8,128)(2,1)S(1)}, u32[]{:S(2)}, u32[]{:S(2)}) async-start(bf16[8,768,256]{1,2,0:T(8,128)(2,1)} %broadcast_in_dim.9), calls=%async_computation.2 | async-start | bytes 6291456 | tf_op jit(solution)/shard_map/all_to_all | solution.py:11
  154.6 0.0 copy-start.12
  154.6 0.1 reduce-scatter.5.cloned.1.call-start
  154.6 0.0 copy-done.20
  154.7 30.6 %all_gather.23 = bf16[1,2048]{1,0:T(2,128)(2,1)S(1)} all-gather(bf16[1,128]{1,0:T(2,128)(2,1)S(1)} %convert_element_type.116), channel_id=1, replica_groups=mesh['grp'=2,'fs'=16,'tp'=8] {'fs'}, dimensions={1}, use_global_device_ids=true | all-gather | bytes 4352 | tf_op jit(solution)/shard_map/all_gather | solution.py:54
  185.3 7.4 %all-to-all-done.1 = bf16[8,768,256]{1,2,0:T(8,128)(2,1)S(1)} async-done(((bf16[8,768,256]{1,2,0:T(8,128)(2,1)}), bf16[8,768,256]{1,2,0:T(8,128)(2,1)S(1)}, u32[]{:S(2)}, u32[]{:S(2)}) %all-to-all-start.1) | async-done | bytes 3145760 | tf_op jit(solution)/shard_map/all_to_all | solution.py:11
  192.7 0.7 multiply_reduce_fusion
  193.4 0.0 copy-done.12
  193.5 2.5 fusion.1
  195.9 59.6 %all-gather.6.cloned.1.call-done = bf16[2048,1408]{0,1:T(8,128)(2,1)} async-done(((bf16[128,1408]{0,1:T(8,128)(2,1)}), bf16[2048,1408]{0,1:T(8,128)(2,1)}) %all-gather.6.cloned.1.call-update) | async-done | bytes 5767184 | tf_op jit(solution)/shard_map/all_gather | solution.py:27
  255.5 6.6 %fusion.4 = f32[768,704]{0,1:T(8,128)} fusion(bf16[768,2048]{0,1:T(8,128)(2,1)} %fusion.1, bf16[2048,1408]{0,1:T(8,128)(2,1)} %all-gather.6.cloned.1.call-done), kind=kOutput, calls=%fused_computation.10 | convolution fusion | flops 2214592512 | bytes 8192000 | tf_op jit(solution)/shard_map/dot_general | solution.py:47
  262.1 72.1 %all-gather.8.cloned.1.call-done = bf16[704,2048]{1,0:T(8,128)(2,1)} async-done(((bf16[704,128]{1,0:T(8,128)(2,1)}), bf16[704,2048]{1,0:T(8,128)(2,1)}) %all-gather.8.cloned.1.call-update) | async-done | bytes 2883600 | tf_op jit(solution)/shard_map/all_gather | solution.py:53
  334.2 11.6 %multiply_convert_fusion = bf16[768,2048]{1,0:T(8,128)(2,1)} fusion(bf16[704,2048]{1,0:T(8,128)(2,1)} %all-gather.8.cloned.1.call-done, f32[2048]{0:T(1024)S(1)} %bitcast.42, f32[768,704]{0,1:T(8,128)} %fusion.4, bf16[768,2048]{0,1:T(8,128)(2,1)S(1)} %copy-done, bf16[2048,1408]{0,1:T(8,128)(2,1)} %all-gather.6.cloned.1.call-done, f32[704]{0:T(1024)S(1)} %copy-done.15, ...), kind=kOutput, calls=%fused_computation.6 | convolution fusion | flops 4436656128 | bytes 14235136 | tf_op jit(solution)/shard_map/dot_general | solution.py:59
  345.8 0.1 reduce-scatter.5.cloned.1.call-update
  345.9 38.4 %reduce-scatter.5.cloned.1.call-done = bf16[768,256]{1,0:T(8,128)(2,1)} async-done(((bf16[768,2048]{1,0:T(8,128)(2,1)}), bf16[768,256]{1,0:T(8,128)(2,1)}) %reduce-scatter.5.cloned.1.call-update) | async-done | bytes 393232 | tf_op jit(solution)/shard_map/reduce_scatter | solution.py:60
  384.3 1.8 add_convert_fusion
  (30 shorter events, 0.1 us)
Async XLA Ops:
  9.6 4.8 %copy-start.7 = (f32[128,128]{1,0:T(8,128)S(1)}, f32[128,128]{1,0:T(8,128)}, u32[]{:S(2)}) copy-start(f32[128,128]{1,0:T(8,128)} %param.19) | copy-start | bytes 196612
  9.6 4.8 %copy-start.8 = (f32[128,128]{1,0:T(8,128)S(1)}, f32[128,128]{1,0:T(8,128)}, u32[]{:S(2)}) copy-start(f32[128,128]{1,0:T(8,128)} %param.20) | copy-start | bytes 196612
  9.6 5.6 %copy-start.17 = (f32[1,128]{1,0:T(1,128)S(1)}, f32[1,128]{1,0:T(1,128)}, u32[]{:S(2)}) copy-start(f32[1,128]{1,0:T(1,128)} %param.26) | copy-start | bytes 1540
  9.6 54.0 %copy-start.9 = (f32[128,128]{1,0:T(8,128)S(1)}, f32[128,128]{1,0:T(8,128)}, u32[]{:S(2)}) copy-start(f32[128,128]{1,0:T(8,128)} %param.25) | copy-start | bytes 196612
  9.6 86.6 %all-to-all-start = ((bf16[8,768,256]{1,2,0:T(8,128)(2,1)}), bf16[8,768,256]{1,2,0:T(8,128)(2,1)S(1)}, u32[]{:S(2)}, u32[]{:S(2)}) async-start(bf16[8,768,256]{1,2,0:T(8,128)(2,1)} %broadcast_in_dim.7), calls=%async_computation | async-start | bytes 6291456 | tf_op jit(solution)/shard_map/all_to_all | solution.py:11
  14.3 82.5 %copy-start.11 = (f32[2048]{0:T(1024)S(1)}, f32[2048]{0:T(1024)}, u32[]{:S(2)}) copy-start(f32[2048]{0:T(1024)} %param.18) | copy-start | bytes 24580
  14.3 85.2 %all-gather.4.cloned.1.call-start = ((), (), s32[]{:S(2)}) async-start(), calls=%async_computation.4 | async-start | bytes 1114112 | tf_op jit(solution)/shard_map/all_gather | solution.py:27
  15.1 132.3 %reduce-scatter.3.cloned.1.call-start = ((), (), s32[]{:S(2)}) async-start(), calls=%async_computation.5 | async-start | bytes 3538944 | tf_op jit(solution)/shard_map/reduce_scatter | solution.py:60
  96.8 2.7 copy-start.18
  99.3 4.2 %copy-start.10 = (bf16[1,128,128]{2,1,0:T(8,128)(2,1)S(1)}, bf16[1,128,128]{2,1,0:T(8,128)(2,1)}, u32[]{:S(2)}) copy-start(bf16[1,128,128]{2,1,0:T(8,128)(2,1)} %param.23) | copy-start | bytes 98308
  99.3 4.2 %copy-start.13 = (f32[1,128]{1,0:T(1,128)S(1)}, f32[1,128]{1,0:T(1,128)}, u32[]{:S(2)}) copy-start(f32[1,128]{1,0:T(1,128)} %param.24) | copy-start | bytes 1540
  99.3 4.4 %copy-start.1 = (bf16[768,2048]{0,1:T(8,128)(2,1)S(1)}, bf16[768,2048]{0,1:T(8,128)(2,1)}, u32[]{:S(2)}) copy-start(bf16[768,2048]{0,1:T(8,128)(2,1)} %fusion.3) | copy-start | bytes 9437188
  99.3 4.4 %copy-start.19 = (f32[128]{0:T(128)S(1)}, f32[128]{0:T(128)}, u32[]{:S(2)}) copy-start(f32[128]{0:T(128)} %param.21) | copy-start | bytes 1540
  99.6 4.1 %copy-start.14 = (bf16[2048,256]{1,0:T(8,128)(2,1)S(1)}, bf16[2048,256]{1,0:T(8,128)(2,1)}, u32[]{:S(2)}) copy-start(bf16[2048,256]{1,0:T(8,128)(2,1)} %all-gather.4.cloned.1.call-done) | copy-start | bytes 3145732
  103.7 1.7 copy-start.2
  105.4 2.8 copy-start.4
  105.4 2.8 copy-start.5
  108.1 1.1 copy-start.6
  108.1 39.3 %copy-start.3 = (bf16[768,256]{1,0:T(8,128)(2,1)S(1)}, bf16[768,256]{1,0:T(8,128)(2,1)}, u32[]{:S(2)}) copy-start(bf16[768,256]{1,0:T(8,128)(2,1)} %param.17) | copy-start | bytes 1179652
  108.2 147.4 %all-gather.6.cloned.1.call-start = ((), (), s32[]{:S(2)}) async-start(), calls=%async_computation.6 | async-start | bytes 6127616 | tf_op jit(solution)/shard_map/all_gather | solution.py:27
  109.1 225.1 %all-gather.8.cloned.1.call-start = ((), (), s32[]{:S(2)}) async-start(), calls=%async_computation.7 | async-start | bytes 3063808 | tf_op jit(solution)/shard_map/all_gather | solution.py:53
  150.6 4.1 %copy-start.20 = (f32[1,128]{1,0:T(1,128)S(1)}, f32[1,128]{1,0:T(1,128)}, u32[]{:S(2)}) copy-start(f32[1,128]{1,0:T(1,128)} %param.33) | copy-start | bytes 1540
  150.6 42.2 %all-to-all-start.1 = ((bf16[8,768,256]{1,2,0:T(8,128)(2,1)}), bf16[8,768,256]{1,2,0:T(8,128)(2,1)S(1)}, u32[]{:S(2)}, u32[]{:S(2)}) async-start(bf16[8,768,256]{1,2,0:T(8,128)(2,1)} %broadcast_in_dim.9), calls=%async_computation.2 | async-start | bytes 6291456 | tf_op jit(solution)/shard_map/all_to_all | solution.py:11
  154.6 38.9 %copy-start.12 = (f32[2048]{0:T(1024)S(1)}, f32[2048]{0:T(1024)}, u32[]{:S(2)}) copy-start(f32[2048]{0:T(1024)} %param.27) | copy-start | bytes 24580
  154.6 229.7 %reduce-scatter.5.cloned.1.call-start = ((), (), s32[]{:S(2)}) async-start(), calls=%async_computation.8 | async-start | bytes 3538944 | tf_op jit(solution)/shard_map/reduce_scatter | solution.py:60
  195.9 138.3 %copy-start = (bf16[768,2048]{0,1:T(8,128)(2,1)S(1)}, bf16[768,2048]{0,1:T(8,128)(2,1)}, u32[]{:S(2)}) copy-start(bf16[768,2048]{0,1:T(8,128)(2,1)} %fusion.1) | copy-start | bytes 9437188
  195.9 138.3 %copy-start.15 = (f32[704]{0:T(1024)S(1)}, f32[704]{0:T(1024)}, u32[]{:S(2)}) copy-start(f32[704]{0:T(1024)} %param.31) | copy-start | bytes 8452
  195.9 138.3 %copy-start.16 = (f32[704]{0:T(1024)S(1)}, f32[704]{0:T(1024)}, u32[]{:S(2)}) copy-start(f32[704]{0:T(1024)} %param.30) | copy-start | bytes 8452
Sparse Core Ops, SparseCore 0:
  16.9 82.5 all-gather.3
  108.3 39.0 reduce-scatter.2
  149.1 106.3 all-gather.5
  257.1 77.0 all-gather.7
  346.0 38.2 reduce-scatter.4
where the time goes:
time: 393 us
  waiting for transfers between devices  216 us (55%)
  blocking collectives  111 us (28%)
  matrix products  26.5 us (7%)
  between operations  13.5 us (3%)
  other arithmetic  11.4 us (3%)
  starting transfers between devices  9.04 us (2%)
  local copies, waits for them, and re-layouts  5.15 us (1%)
    all_gather x2, blocking collectives, collect_out(): lax.all_gather(scale.astype(jnp.bfloat16), 'fs', axis=1, tiled=True)  79 us
    reduce_scatter x2, waiting for transfers between devices, reduce_out(): lax.psum_scatter(term.astype(jnp.bfloat16), 'tp', scatter_dimension=1, ti...  75.9 us
    all_gather x1, waiting for transfers between devices, collect_out(): lax.all_gather(weight.astype(jnp.bfloat16), 'fs', axis=1, tiled=True)  72.1 us
    all_gather x2, waiting for transfers between devices, in_one_piece(): out, at, done = (lax.all_gather(both, axis, axis=dim, tiled=True), 0, [])  59.9 us
    all_gather x1, blocking collectives, collect_out(): lax.all_gather(weight.astype(jnp.bfloat16), 'fs', axis=1, tiled=True)  32.5 us
    dot_general x2, matrix products, reduce_out(): term = jnp.dot(hidden, weight, preferred_element_type=jnp.float32) * scale  14.2 us
    dot_general x2, matrix products, project_pair(): jnp.dot(rows, pieces[1], preferred_element_type=jnp.float32)  10.4 us
    all_to_all x2, starting transfers between devices, sent_to_all(): lax.all_to_all(jnp.broadcast_to(x[None], (count, *x.shape)), axis, 0, 0,...  8.72 us
  transfers between devices with their start and end apart: 7, of which 6 were waited for; matrix products, arithmetic and copies ran while one was open for 5% of the time, Pallas kernels for 0%

commit v1 on v0

--- a/solution.py
+++ b/solution.py
@@ -49,8 +49,16 @@
 
 
 def collect_out(weight, scale):
+
+    def _test_sizes(values):
+        arr_next = jnp.concatenate(
+            lax.all_to_all(jnp.stack([values for _ in range(lax.axis_size("fs"))], 0), "fs", 0, 0),
+            axis=1,
+        )
+        return arr_next
+
     return (
-        lax.all_gather(weight.astype(jnp.bfloat16), "fs", axis=1, tiled=True),
+        _test_sizes(weight.astype(jnp.bfloat16)),
         lax.all_gather(scale.astype(jnp.bfloat16), "fs", axis=1, tiled=True).astype(scale.dtype),
     )
 

time: 393 us -> 456 us (1.16)
  blocking collectives: 111 us -> 218 us
  waiting for transfers between devices: 216 us -> 139 us
  starting transfers between devices: 9.04 us -> 34.4 us
    all_gather x2, blocking collectives: 79 us -> 218 us  [collect_out(): lax.all_gather(scale.astype(jnp.bfloat16), 'fs', axis=1, tiled=True)]
    all_gather x1 -> x0, waiting for transfers between devices: 72.1 us -> none  [collect_out(): lax.all_gather(weight.astype(jnp.bfloat16), 'fs', axis=1, tiled=True)]
    all_gather x2, waiting for transfers between devices: 59.9 us -> 26.7 us  [in_one_piece(): out, at, done = (lax.all_gather(both, axis, axis=dim, tiled=True), 0, [])]
    all_gather x1 -> x0, blocking collectives: 32.5 us -> none  [collect_out(): lax.all_gather(weight.astype(jnp.bfloat16), 'fs', axis=1, tiled=True)]
    all_to_all x2, waiting for transfers between devices: 7.44 us -> 33.6 us  [sent_to_all(): lax.all_to_all(jnp.broadcast_to(x[None], (count, *x.shape)), axis, 0, 0,...]
    all_to_all x0 -> x2, starting transfers between devices: none -> 25.5 us  [_test_sizes(): lax.all_to_all(jnp.stack([values for _ in range(lax.axis_size('fs'))], 0)...]
  transfers between devices with their start and end apart: 7 -> 8, of which waited for: 6 -> 4; matrix products, arithmetic and copies ran while one was open for 5% -> 6% of each run, Pallas kernels for 0% -> 0%
where the time goes in v1:
time: 456 us
  blocking collectives  218 us (48%)
  waiting for transfers between devices  139 us (30%)
  starting transfers between devices  34.4 us (8%)
  matrix products  27.6 us (6%)
  other arithmetic  14.3 us (3%)
  between operations  13.4 us (3%)
  local copies, waits for them, and re-layouts  9.25 us (2%)
    all_gather x2, blocking collectives, collect_out(): lax.all_gather(scale.astype(jnp.bfloat16), 'fs', axis=1, tiled=True)  218 us
    reduce_scatter x2, waiting for transfers between devices, reduce_out(): lax.psum_scatter(term.astype(jnp.bfloat16), 'tp', scatter_dimension=1, ti...  78.2 us
    all_to_all x2, waiting for transfers between devices, sent_to_all(): lax.all_to_all(jnp.broadcast_to(x[None], (count, *x.shape)), axis, 0, 0,...  33.6 us
    all_gather x2, waiting for transfers between devices, in_one_piece(): out, at, done = (lax.all_gather(both, axis, axis=dim, tiled=True), 0, [])  26.7 us
    all_to_all x2, starting transfers between devices, _test_sizes(): lax.all_to_all(jnp.stack([values for _ in range(lax.axis_size('fs'))], 0)...  25.5 us
    dot_general x2, matrix products, reduce_out(): term = jnp.dot(hidden, weight, preferred_element_type=jnp.float32) * scale  15.2 us
    dot_general x2, matrix products, project_pair(): jnp.dot(rows, pieces[1], preferred_element_type=jnp.float32)  10.4 us
  transfers between devices with their start and end apart: 8, of which 4 were waited for; matrix products, arithmetic and copies ran while one was open for 6% of the time, Pallas kernels for 0%

profile of v1, /device:TPU:40, one launch (start us, length us, event | category | flops | bytes accessed | tf_op | source)
XLA Modules:
  0.0 455.5 jit_solution(3014302320409553870)
XLA Ops:
  6.5 1.2 copy.21
  7.7 1.8 broadcast_in_dim.7
  9.6 4.7 %all-to-all-start = ((bf16[8,768,256]{1,2,0:T(8,128)(2,1)}), bf16[8,768,256]{1,2,0:T(8,128)(2,1)S(1)}, u32[]{:S(2)}, u32[]{:S(2)}) async-start(bf16[8,768,256]{1,2,0:T(8,128)(2,1)} %broadcast_in_dim.7), calls=%async_computation | async-start | bytes 6291456 | tf_op jit(solution)/shard_map/all_to_all | solution.py:11
  14.3 0.1 all-gather.3.cloned.1.call-start
  14.4 0.0 copy-done.3
  14.4 0.0 copy-done.4
  14.4 0.6 pad_maximum_fusion.1
  15.1 0.1 all-gather.3.cloned.1.call-update
  15.1 0.0 copy-done.13
  15.1 48.4 %all_gather.13 = bf16[1,2048]{1,0:T(2,128)(2,1)S(1)} all-gather(bf16[1,128]{1,0:T(2,128)(2,1)S(1)} %convert_element_type.102), channel_id=1, replica_groups=mesh['grp'=2,'fs'=16,'tp'=8] {'fs'}, dimensions={1}, use_global_device_ids=true | all-gather | bytes 4352 | tf_op jit(solution)/shard_map/all_gather | solution.py:62
  63.5 0.0 copy-done.5
  63.5 0.1 copy.22
  63.6 0.0 all-to-all-done
  63.7 0.9 stack.4
  64.6 13.0 %all-to-all-start.1 = ((bf16[16,128,128]{1,2,0:T(8,128)(2,1)}), bf16[16,128,128]{1,2,0:T(8,128)(2,1)}, u32[]{:S(2)}, u32[]{:S(2)}) async-start(bf16[16,128,128]{1,2,0:T(8,128)(2,1)} %stack.4), calls=%async_computation.1 | async-start | bytes 1048576 | tf_op jit(solution)/shard_map/all_to_all | solution.py:55
  77.6 0.1 reduce-scatter.3.cloned.1.call-start
  77.7 0.7 multiply_reduce_fusion.1
  78.4 0.0 copy-done.7
  78.4 0.0 copy-start.14
  78.4 2.4 fusion.3
  80.8 26.7 %all-gather.3.cloned.1.call-done = bf16[2048,256]{1,0:T(8,128)(2,1)} async-done(((bf16[128,256]{1,0:T(8,128)(2,1)}), bf16[2048,256]{1,0:T(8,128)(2,1)}) %all-gather.3.cloned.1.call-update) | async-done | bytes 1048592 | tf_op jit(solution)/shard_map/all_gather | solution.py:27
  107.5 0.0 copy-done.14
  107.5 3.8 fusion.23
  111.3 0.0 copy-done.6
  111.3 0.0 copy-done.9
  111.3 0.2 fusion.12
  111.5 0.0 copy-done.1
  111.5 0.0 copy-done.15
  111.5 0.0 copy-done.10
  111.5 1.7 fusion.20
  113.3 0.0 all-to-all-done.1
  113.3 0.0 copy-start.2
  113.3 3.7 multiply_convert_fusion.1
  117.0 0.1 reduce-scatter.3.cloned.1.call-update
  117.1 40.1 %reduce-scatter.3.cloned.1.call-done = bf16[768,256]{1,0:T(8,128)(2,1)} async-done(((bf16[768,2048]{1,0:T(8,128)(2,1)}), bf16[768,256]{1,0:T(8,128)(2,1)}) %reduce-scatter.3.cloned.1.call-update) | async-done | bytes 393232 | tf_op jit(solution)/shard_map/reduce_scatter | solution.py:68
  157.2 0.0 copy-done.2
  157.2 1.1 add_convert_fusion.1
  158.3 0.2 copy.23
  158.4 1.9 broadcast_in_dim.9
  160.3 3.9 all-to-all-start.2
  164.2 0.1 all-gather.5.cloned.1.call-start
  164.3 1.0 convert_element_type.112
  165.3 1.0 convert_element_type.113
  166.3 0.8 pad_maximum_fusion
  167.0 0.1 all-gather.5.cloned.1.call-update
  167.1 1.7 convert_element_type.115
  168.8 33.6 %all-to-all-done.2 = bf16[8,768,256]{1,2,0:T(8,128)(2,1)S(1)} async-done(((bf16[8,768,256]{1,2,0:T(8,128)(2,1)}), bf16[8,768,256]{1,2,0:T(8,128)(2,1)S(1)}, u32[]{:S(2)}, u32[]{:S(2)}) %all-to-all-start.2) | async-done | bytes 3145760 | tf_op jit(solution)/shard_map/all_to_all | solution.py:11
  202.4 3.1 stack.5
  205.5 12.5 %all-to-all-start.3 = ((bf16[16,704,128]{2,1,0:T(8,128)(2,1)}), bf16[16,704,128]{2,1,0:T(8,128)(2,1)}, u32[]{:S(2)}, u32[]{:S(2)}) async-start(bf16[16,704,128]{2,1,0:T(8,128)(2,1)} %stack.5), calls=%async_computation.4 | async-start | bytes 5767168 | tf_op jit(solution)/shard_map/all_to_all | solution.py:55
  218.0 0.1 reduce-scatter.5.cloned.1.call-start
  218.1 0.0 copy-done.16
  218.1 169.6 %all_gather.15 = bf16[1,2048]{1,0:T(2,128)(2,1)S(1)} all-gather(bf16[1,128]{1,0:T(2,128)(2,1)S(1)} %convert_element_type.116), channel_id=1, replica_groups=mesh['grp'=2,'fs'=16,'tp'=8] {'fs'}, dimensions={1}, use_global_device_ids=true | all-gather | bytes 4352 | tf_op jit(solution)/shard_map/all_gather | solution.py:62
  387.7 0.7 multiply_reduce_fusion
  388.4 0.0 copy-done.8
  388.4 2.5 fusion.1
  390.8 6.6 %fusion.6 = f32[768,704]{0,1:T(8,128)} fusion(bf16[768,2048]{0,1:T(8,128)(2,1)} %fusion.1, bf16[2048,1408]{0,1:T(8,128)(2,1)} %all-gather.5.cloned.1.call-done), kind=kOutput, calls=%fused_computation.12 | convolution fusion | flops 2214592512 | bytes 8192000 | tf_op jit(solution)/shard_map/dot_general | solution.py:47
  397.5 0.0 all-to-all-done.3
  397.5 0.0 copy-done
  397.5 0.0 copy-done.11
  397.5 0.0 copy-done.12
  397.5 11.5 %multiply_convert_fusion = bf16[768,2048]{1,0:T(8,128)(2,1)} fusion(f32[2048]{0:T(1024)S(1)} %bitcast.52, f32[768,704]{0,1:T(8,128)} %fusion.6, bf16[768,2048]{0,1:T(8,128)(2,1)S(1)} %copy-done, bf16[2048,1408]{0,1:T(8,128)(2,1)} %all-gather.5.cloned.1.call-done, f32[704]{0:T(1024)S(1)} %copy-done.11, f32[704]{0:T(1024)S(1)} %copy-done.12, ...), kind=kOutput, calls=%fused_computation.6 | convolution fusion | flops 4436656128 | bytes 14235136 | tf_op jit(solution)/shard_map/dot_general | solution.py:67
  409.0 0.1 reduce-scatter.5.cloned.1.call-update
  409.1 38.1 %reduce-scatter.5.cloned.1.call-done = bf16[768,256]{1,0:T(8,128)(2,1)} async-done(((bf16[768,2048]{1,0:T(8,128)(2,1)}), bf16[768,256]{1,0:T(8,128)(2,1)}) %reduce-scatter.5.cloned.1.call-update) | async-done | bytes 393232 | tf_op jit(solution)/shard_map/reduce_scatter | solution.py:68
  447.2 1.8 add_convert_fusion
  (25 shorter events, 0.1 us)
Async XLA Ops:
  9.6 4.8 %copy-start.3 = (f32[128,128]{1,0:T(8,128)S(1)}, f32[128,128]{1,0:T(8,128)}, u32[]{:S(2)}) copy-start(f32[128,128]{1,0:T(8,128)} %param.19) | copy-start | bytes 196612
  9.6 4.8 %copy-start.4 = (f32[128,128]{1,0:T(8,128)S(1)}, f32[128,128]{1,0:T(8,128)}, u32[]{:S(2)}) copy-start(f32[128,128]{1,0:T(8,128)} %param.20) | copy-start | bytes 196612
  9.6 5.6 %copy-start.13 = (f32[1,128]{1,0:T(1,128)S(1)}, f32[1,128]{1,0:T(1,128)}, u32[]{:S(2)}) copy-start(f32[1,128]{1,0:T(1,128)} %param.26) | copy-start | bytes 1540
  9.6 53.9 %copy-start.5 = (f32[128,128]{1,0:T(8,128)S(1)}, f32[128,128]{1,0:T(8,128)}, u32[]{:S(2)}) copy-start(f32[128,128]{1,0:T(8,128)} %param.25) | copy-start | bytes 196612
  9.6 54.1 %all-to-all-start = ((bf16[8,768,256]{1,2,0:T(8,128)(2,1)}), bf16[8,768,256]{1,2,0:T(8,128)(2,1)S(1)}, u32[]{:S(2)}, u32[]{:S(2)}) async-start(bf16[8,768,256]{1,2,0:T(8,128)(2,1)} %broadcast_in_dim.7), calls=%async_computation | async-start | bytes 6291456 | tf_op jit(solution)/shard_map/all_to_all | solution.py:11
  14.3 64.1 %copy-start.7 = (f32[2048]{0:T(1024)S(1)}, f32[2048]{0:T(1024)}, u32[]{:S(2)}) copy-start(f32[2048]{0:T(1024)} %param.18) | copy-start | bytes 24580
  14.3 93.2 %all-gather.3.cloned.1.call-start = ((), (), s32[]{:S(2)}) async-start(), calls=%async_computation.6 | async-start | bytes 1114112 | tf_op jit(solution)/shard_map/all_gather | solution.py:27
  64.6 48.7 %all-to-all-start.1 = ((bf16[16,128,128]{1,2,0:T(8,128)(2,1)}), bf16[16,128,128]{1,2,0:T(8,128)(2,1)}, u32[]{:S(2)}, u32[]{:S(2)}) async-start(bf16[16,128,128]{1,2,0:T(8,128)(2,1)} %stack.4), calls=%async_computation.1 | async-start | bytes 1048576 | tf_op jit(solution)/shard_map/all_to_all | solution.py:55
  77.6 79.6 %reduce-scatter.3.cloned.1.call-start = ((), (), s32[]{:S(2)}) async-start(), calls=%async_computation.7 | async-start | bytes 3538944 | tf_op jit(solution)/shard_map/reduce_scatter | solution.py:68
  78.4 29.1 %copy-start.14 = (f32[128]{0:T(128)S(1)}, f32[128]{0:T(128)}, u32[]{:S(2)}) copy-start(f32[128]{0:T(128)} %param.22) | copy-start | bytes 1540
  80.8 30.5 %copy-start.6 = (bf16[1,128,128]{2,1,0:T(8,128)(2,1)S(1)}, bf16[1,128,128]{2,1,0:T(8,128)(2,1)}, u32[]{:S(2)}) copy-start(bf16[1,128,128]{2,1,0:T(8,128)(2,1)} %param.23) | copy-start | bytes 98308
  80.8 30.5 %copy-start.9 = (f32[1,128]{1,0:T(1,128)S(1)}, f32[1,128]{1,0:T(1,128)}, u32[]{:S(2)}) copy-start(f32[1,128]{1,0:T(1,128)} %param.24) | copy-start | bytes 1540
  80.8 30.7 %copy-start.1 = (bf16[768,2048]{0,1:T(8,128)(2,1)S(1)}, bf16[768,2048]{0,1:T(8,128)(2,1)}, u32[]{:S(2)}) copy-start(bf16[768,2048]{0,1:T(8,128)(2,1)} %fusion.3) | copy-start | bytes 9437188
  80.8 30.7 %copy-start.15 = (f32[128]{0:T(128)S(1)}, f32[128]{0:T(128)}, u32[]{:S(2)}) copy-start(f32[128]{0:T(128)} %param.21) | copy-start | bytes 1540
  107.5 4.0 copy-start.10
  113.3 43.9 %copy-start.2 = (bf16[768,256]{1,0:T(8,128)(2,1)S(1)}, bf16[768,256]{1,0:T(8,128)(2,1)}, u32[]{:S(2)}) copy-start(bf16[768,256]{1,0:T(8,128)(2,1)} %param.17) | copy-start | bytes 1179652
  160.3 42.0 %all-to-all-start.2 = ((bf16[8,768,256]{1,2,0:T(8,128)(2,1)}), bf16[8,768,256]{1,2,0:T(8,128)(2,1)S(1)}, u32[]{:S(2)}, u32[]{:S(2)}) async-start(bf16[8,768,256]{1,2,0:T(8,128)(2,1)} %broadcast_in_dim.9), calls=%async_computation.3 | async-start | bytes 6291456 | tf_op jit(solution)/shard_map/all_to_all | solution.py:11
  164.2 226.6 %all-gather.5.cloned.1.call-start = ((), (), s32[]{:S(2)}) async-start(), calls=%async_computation.8 | async-start | bytes 6127616 | tf_op jit(solution)/shard_map/all_gather | solution.py:27
  205.5 12.6 %copy-start.16 = (f32[1,128]{1,0:T(1,128)S(1)}, f32[1,128]{1,0:T(1,128)}, u32[]{:S(2)}) copy-start(f32[1,128]{1,0:T(1,128)} %param.33) | copy-start | bytes 1540
  205.5 182.9 %copy-start.8 = (f32[2048]{0:T(1024)S(1)}, f32[2048]{0:T(1024)}, u32[]{:S(2)}) copy-start(f32[2048]{0:T(1024)} %param.27) | copy-start | bytes 24580
  205.5 192.0 %all-to-all-start.3 = ((bf16[16,704,128]{2,1,0:T(8,128)(2,1)}), bf16[16,704,128]{2,1,0:T(8,128)(2,1)}, u32[]{:S(2)}, u32[]{:S(2)}) async-start(bf16[16,704,128]{2,1,0:T(8,128)(2,1)} %stack.5), calls=%async_computation.4 | async-start | bytes 5767168 | tf_op jit(solution)/shard_map/all_to_all | solution.py:55
  218.0 229.2 %reduce-scatter.5.cloned.1.call-start = ((), (), s32[]{:S(2)}) async-start(), calls=%async_computation.9 | async-start | bytes 3538944 | tf_op jit(solution)/shard_map/reduce_scatter | solution.py:68
  390.8 6.7 %copy-start = (bf16[768,2048]{0,1:T(8,128)(2,1)S(1)}, bf16[768,2048]{0,1:T(8,128)(2,1)}, u32[]{:S(2)}) copy-start(bf16[768,2048]{0,1:T(8,128)(2,1)} %fusion.1) | copy-start | bytes 9437188
  390.8 6.7 %copy-start.11 = (f32[704]{0:T(1024)S(1)}, f32[704]{0:T(1024)}, u32[]{:S(2)}) copy-start(f32[704]{0:T(1024)} %param.31) | copy-start | bytes 8452
  390.8 6.7 %copy-start.12 = (f32[704]{0:T(1024)S(1)}, f32[704]{0:T(1024)}, u32[]{:S(2)}) copy-start(f32[704]{0:T(1024)} %param.30) | copy-start | bytes 8452
Sparse Core Ops, SparseCore 0:
  16.9 90.5 all-gather.2
  117.2 39.9 reduce-scatter.2
  167.2 222.7 all-gather.4
  409.2 37.8 reduce-scatter.4
